TPU v7x, 32 devices: a whole 2x2x4 slice. The times are simulated.
32 devices in a mesh: ep: 8 (over z, x), tp: 4 (over y, core).
Axes of the slice: x: 2, y: 2, z: 4, core: 2. Of those that a mesh axis runs over, the one named last changes fastest.
Arguments:
- tokens: bfloat16 [768, 4096], P('ep'), may hold values from -6 to 6
- mix_gain: float32 [4096], replicated, may hold values from 0.1 to 1.9
- ffn_gain: float32 [4096], replicated, may hold values from 0.1 to 1.9
- in_proj: bfloat16 [4096, 1024], P(None, 'tp'), may hold values from -0.09375 to 0.09375
- decay_rate: float32 [64, 64], P('tp'), may hold values from 0.05 to 2
- frequency: float32 [64, 64], P('tp'), may hold values from -3 to 3
- log_step: float32 [64], P('tp'), may hold values from -3 to 0.5
- b_real: float32 [64, 64, 16], P('tp'), may hold values from -1.5 to 1.5
- b_imag: float32 [64, 64, 16], P('tp'), may hold values from -1.5 to 1.5
- c_real: float32 [64, 16, 64], P('tp'), may hold values from -0.75 to 0.75
- c_imag: float32 [64, 16, 64], P('tp'), may hold values from -0.75 to 0.75
- skip_gain: float32 [1024], P('tp'), may hold values from -5 to 5
- states: float32 [2, 768, 4096], P(None, 'ep', 'tp'), may hold values from -6 to 6
- out_proj: bfloat16 [1024, 4096], P('tp'), may hold values from -0.1875 to 0.1875
- route_ids: int32 [768, 2], P('ep'), may hold values from 0 to 7, all different within a row; in each aligned block of 96 rows (0 to 95, 96 to 191, ...) at most 48 rows name the same one
- route_logits: float32 [768, 2], P('ep'), may hold values from -5 to 5
- expert_gate: bfloat16 [8, 4096, 3072], P('ep', None, 'tp'), may hold values from -0.09375 to 0.09375
- expert_up: bfloat16 [8, 4096, 3072], P('ep', None, 'tp'), may hold values from -0.09375 to 0.09375
- expert_down: bfloat16 [8, 3072, 4096], P('ep', 'tp'), may hold values from -0.109375 to 0.109375
- dense_gate: bfloat16 [4096, 6144], P('tp', 'ep'), may hold values from -0.09375 to 0.09375
- dense_up: bfloat16 [4096, 6144], P('tp', 'ep'), may hold values from -0.09375 to 0.09375
- dense_down: bfloat16 [6144, 4096], P('ep', 'tp'), may hold values from -0.078125 to 0.078125
- branch_gate: bfloat16 [4096], replicated, may hold values from -0.09375 to 0.09375
Outputs:
- output: bfloat16 [768, 4096], P('ep', 'tp')
- new_states: float32 [2, 768, 4096], P(None, 'ep', 'tp')
Inputs may be any that keep to these rules, and one draw needn't show every extreme that they name: `route_ids`: each row names 2 different experts; among the rows of one device (aligned blocks of 96 rows) no expert is named by more than 48 rows.
All inputs are finite; a program needn't handle non-finite values.
Results may differ from a plain program's by a relative error of at most 0.017.
Values may be sent and summed in bfloat16 or wider, within the bound.
A program may use at most 128 MiB of HBM per device.

v0:
```python
import jax
import jax.numpy as jnp
from jax import lax
from jax.sharding import PartitionSpec as P

GROUP = 16
STATE = 64


def rms_norm(values, gain):
    flt = values.astype(jnp.float32)
    scaled = flt * lax.rsqrt(jnp.mean(flt * flt, axis=-1, keepdims=True) + 1e-06)
    return (scaled * gain).astype(jnp.bfloat16)


def discretize(decay_rate, frequency, log_step, b_real, b_imag):
    step_size = jnp.exp(log_step)[:, None]
    lam_re = -decay_rate
    magnitude = jnp.exp(lam_re * step_size)
    abar_re = magnitude * jnp.cos(frequency * step_size)
    abar_im = magnitude * jnp.sin(frequency * step_size)
    denom = lam_re * lam_re + frequency * frequency
    fac_re = ((abar_re - 1.0) * lam_re + abar_im * frequency) / denom
    fac_im = (abar_im * lam_re - (abar_re - 1.0) * frequency) / denom
    bbar_re = fac_re[..., None] * b_real - fac_im[..., None] * b_imag
    bbar_im = fac_re[..., None] * b_imag + fac_im[..., None] * b_real
    return (abar_re, abar_im, bbar_re, bbar_im)


def state_step(
    drive, states, decay_rate, frequency, log_step, b_real, b_imag, c_real, c_imag, skip_gain
):
    count = drive.shape[0]
    groups = decay_rate.shape[0]
    abar_re, abar_im, bbar_re, bbar_im = discretize(decay_rate, frequency, log_step, b_real, b_imag)
    grouped = drive.astype(jnp.float32).reshape(count, groups, GROUP)
    old_re = states[0].reshape(count, groups, STATE)
    old_im = states[1].reshape(count, groups, STATE)
    high = lax.Precision.HIGHEST
    push_re = jnp.einsum("ngh,gph->ngp", grouped, bbar_re, precision=high)
    push_im = jnp.einsum("ngh,gph->ngp", grouped, bbar_im, precision=high)
    new_re = abar_re * old_re - abar_im * old_im + push_re
    new_im = abar_re * old_im + abar_im * old_re + push_im
    readout = (
        jnp.einsum("ngp,ghp->ngh", new_re, c_real, precision=high)
        - jnp.einsum("ngp,ghp->ngh", new_im, c_imag, precision=high)
        + skip_gain.reshape(groups, GROUP) * grouped
    )
    reads = jax.nn.gelu(readout.reshape(count, groups * GROUP)).astype(jnp.bfloat16)
    fresh = jnp.stack(
        [new_re.reshape(count, groups * STATE), new_im.reshape(count, groups * STATE)]
    )
    return (reads, fresh)


def expert_rows(full_rows, gate_w, up_w, down_w, part_width):
    sources, items, width = full_rows.shape
    flat_rows = full_rows.reshape(sources * items, width)
    gate_val = jnp.dot(flat_rows, gate_w, preferred_element_type=jnp.float32)
    up_val = jnp.dot(flat_rows, up_w, preferred_element_type=jnp.float32)
    hidden = (jax.nn.silu(gate_val) * up_val).astype(jnp.bfloat16)
    partial_value = (
        jnp.dot(hidden, down_w, preferred_element_type=jnp.float32)
        .astype(jnp.bfloat16)
        .astype(jnp.float32)
    )
    summed = lax.psum_scatter(
        partial_value.astype(jnp.bfloat16), "tp", scatter_dimension=1, tiled=True
    )
    return summed.reshape(sources, items, part_width)


def shards(
    tokens,
    mix_gain,
    ffn_gain,
    in_proj,
    decay_rate,
    frequency,
    log_step,
    b_real,
    b_imag,
    c_real,
    c_imag,
    skip_gain,
    states,
    out_proj,
    route_ids,
    route_logits,
    expert_gate,
    expert_up,
    expert_down,
    dense_gate,
    dense_up,
    dense_down,
    branch_gate,
):
    seq_count, width = tokens.shape
    tp_count = lax.axis_size("tp")
    ep_count = lax.axis_size("ep")
    tp_index = lax.axis_index("tp")
    part_width = width // tp_count
    normed = rms_norm(tokens, mix_gain)
    drive = jnp.dot(normed, in_proj, preferred_element_type=jnp.float32).astype(jnp.bfloat16)
    reads, new_states = state_step(
        drive, states, decay_rate, frequency, log_step, b_real, b_imag, c_real, c_imag, skip_gain
    )
    partial_value = (
        jnp.dot(reads, out_proj, preferred_element_type=jnp.float32)
        .astype(jnp.bfloat16)
        .astype(jnp.float32)
    )
    mixed = lax.psum(partial_value.astype(jnp.bfloat16), "tp")
    resid = (tokens.astype(jnp.float32) + mixed.astype(jnp.float32)).astype(jnp.bfloat16)
    normed_two = rms_norm(resid, ffn_gain)
    own_cols = lax.dynamic_slice_in_dim(normed_two, tp_index * part_width, part_width, 1)
    hidden_width = dense_gate.shape[1]
    both_proj = jnp.concatenate([dense_gate, dense_up], axis=1)
    partial_both = jnp.dot(
        lax.all_gather(own_cols, "ep", axis=0, tiled=True),
        both_proj,
        preferred_element_type=jnp.float32,
    )
    summed_both = lax.psum(partial_both.astype(jnp.bfloat16), "tp").astype(jnp.float32)
    dense_hidden = (
        jax.nn.silu(summed_both[:, :hidden_width]) * summed_both[:, hidden_width:]
    ).astype(jnp.bfloat16)
    dense_term = lax.psum_scatter(
        jnp.dot(dense_hidden, dense_down, preferred_element_type=jnp.float32).astype(jnp.bfloat16),
        "ep",
        scatter_dimension=0,
        tiled=True,
    ).astype(jnp.float32)
    top_count = route_ids.shape[1]
    capacity = max(2, 2 * seq_count * top_count // ep_count)
    flat_ids = route_ids.reshape(-1)
    onehot = (flat_ids[:, None] == jnp.arange(ep_count, dtype=jnp.int32)[None, :]).astype(jnp.int32)
    rank = jnp.cumsum(onehot, axis=0) - onehot
    slot = jnp.sum(rank * onehot, axis=1)
    target = flat_ids * capacity + slot
    select = target[None, :] == jnp.arange(ep_count * capacity, dtype=jnp.int32)[:, None]
    select = jnp.any(select.reshape(ep_count * capacity, seq_count, top_count), axis=2).astype(
        jnp.bfloat16
    )
    send_rows = jnp.dot(select, normed_two, preferred_element_type=jnp.float32).astype(jnp.bfloat16)
    send_rows = send_rows.reshape(ep_count, capacity, width)
    send_part = lax.dynamic_slice_in_dim(send_rows, tp_index * part_width, part_width, 2)
    full_rows = lax.all_gather(
        lax.all_to_all(send_part, "ep", split_axis=0, concat_axis=0, tiled=True),
        "tp",
        axis=2,
        tiled=True,
    )
    answered = expert_rows(full_rows, expert_gate[0], expert_up[0], expert_down[0], part_width)
    returned = lax.all_to_all(answered, "ep", split_axis=0, concat_axis=0, tiled=True)
    picked_rows = returned.reshape(ep_count * capacity, part_width)[target]
    picked_rows = picked_rows.reshape(seq_count, top_count, part_width).astype(jnp.float32)
    route_weights = jax.nn.softmax(route_logits, axis=-1)
    routed = jnp.sum(route_weights[..., None] * picked_rows, axis=1)
    branch = jax.nn.sigmoid(jnp.dot(normed_two, branch_gate, preferred_element_type=jnp.float32))
    resid_cols = lax.dynamic_slice_in_dim(resid, tp_index * part_width, part_width, 1).astype(
        jnp.float32
    )
    output = (resid_cols + routed + branch[:, None] * dense_term).astype(jnp.bfloat16)
    return (output, new_states)


def solution(mesh):
    return jax.shard_map(
        shards,
        mesh=mesh,
        in_specs=(
            P("ep", None),
            P(),
            P(),
            P(None, "tp"),
            P("tp", None),
            P("tp", None),
            P("tp"),
            P("tp", None, None),
            P("tp", None, None),
            P("tp", None, None),
            P("tp", None, None),
            P("tp"),
            P(None, "ep", "tp"),
            P("tp", None),
            P("ep", None),
            P("ep", None),
            P("ep", None, "tp"),
            P("ep", None, "tp"),
            P("ep", "tp", None),
            P("tp", "ep"),
            P("tp", "ep"),
            P("ep", "tp"),
            P(),
        ),
        out_specs=(P("ep", "tp"), P(None, "ep", "tp")),
        check_vma=False,
    )
```

profile of v0, /device:TPU:0, one launch (start us, length us, event | category | flops | bytes accessed | tf_op | source)
XLA Modules:
  0.0 329.4 jit_solution(16527740815774029400)
XLA Ops:
  7.2 1.4 exp.20
  8.7 2.1 fusion.69
  10.7 1.2 copy.42
  11.9 2.2 copy.43
  14.1 0.3 fusion.16
  14.4 2.8 convolution_convert_fusion.4
  17.2 0.9 copy.44
  18.1 0.8 add_divide_fusion
  18.9 1.9 fusion.26
  20.9 2.2 fusion.27
  23.1 1.5 fusion.70
  24.6 1.5 fusion.30
  26.2 1.4 convolution_convert_fusion.1
  27.7 0.1 eq.36
  27.9 37.6 %all-reduce.4.cloned.1.call-done = bf16[96,4096]{1,0:T(8,128)(2,1)} async-done(((bf16[96,4096]{1,0:T(8,128)(2,1)}), bf16[96,4096]{1,0:T(8,128)(2,1)}) %all-reduce.4.cloned.1.call-update) | async-done | bytes 786448 | tf_op jit(solution)/shard_map/psum | solution.py:113
  65.5 1.7 fusion.13
  67.3 0.9 copy-done.4
  68.1 0.3 fusion.15
  68.4 0.8 constant_dynamic-slice_fusion
  69.3 0.6 reduce-window.6
  69.9 0.2 slice_reduce_fusion
  70.3 0.6 copy-done.9
  70.8 0.8 reduce_sum.52
  71.6 0.8 broadcast_multiply_fusion
  72.6 1.0 convolution_convert_fusion
  73.7 30.8 %all_to_all.10 = bf16[8,48,1024]{2,1,0:T(8,128)(2,1)} all-to-all(bf16[8,48,1024]{2,1,0:T(8,128)(2,1)S(1)} %constant_dynamic-slice_fusion.1), channel_id=1, replica_groups=mesh['ep'=8,'tp'=4] {'ep'}, dimensions={0} | all-to-all | bytes 1572864 | tf_op jit(solution)/shard_map/all_to_all | solution.py:149
  104.6 14.9 %all-gather.5.cloned.1.call-done = bf16[768,1024]{1,0:T(8,128)(2,1)} async-done(((bf16[96,1024]{1,0:T(8,128)(2,1)}), bf16[768,1024]{1,0:T(8,128)(2,1)}) %all-gather.5.cloned.1.call-update) | async-done | bytes 1572880 | tf_op jit(solution)/shard_map/all_gather | solution.py:120
  119.5 6.4 %convolution_convert_fusion.2 = bf16[768,1536]{1,0:T(8,128)(2,1)} fusion(bf16[768,1024]{1,0:T(8,128)(2,1)} %all-gather.5.cloned.1.call-done, bf16[1024,768]{1,0:T(8,128)(2,1)} %param.43, bf16[1024,768]{1,0:T(8,128)(2,1)} %param.42), kind=kOutput, calls=%fused_computation.10 | convolution fusion | flops 2423390208 | bytes 7077888 | tf_op jit(solution)/shard_map/dot_general | solution.py:119
  125.9 0.2 reduce-scatter.3.cloned.1.call-start
  126.1 22.0 %all-gather.3.cloned.1.call-done = bf16[8,48,4096]{2,1,0:T(8,128)(2,1)} async-done(((bf16[8,48,1024]{2,1,0:T(8,128)(2,1)}), bf16[8,48,4096]{2,1,0:T(8,128)(2,1)}) %all-gather.3.cloned.1.call-update) | async-done | bytes 3145744 | tf_op jit(solution)/shard_map/all_gather | solution.py:148
  148.1 7.4 %fusion.4 = f32[384,768]{1,0:T(8,128)} fusion(bf16[384,4096]{1,0:T(8,128)(2,1)} %bitcast.89, bf16[1,4096,768]{2,1,0:T(8,128)(2,1)} %param.39), kind=kOutput, calls=%fused_computation.5 | convolution fusion | flops 2415919104 | bytes 10616832 | tf_op jit(solution)/shard_map/dot_general | solution.py:59
  155.5 14.3 %fusion.6 = bf16[384,4096]{1,0:T(8,128)(2,1)} fusion(bf16[1,768,4096]{2,1,0:T(8,128)(2,1)} %param.41, bf16[384,4096]{1,0:T(8,128)(2,1)} %bitcast.90, bf16[1,4096,768]{2,1,0:T(8,128)(2,1)} %param.40, f32[384,768]{1,0:T(8,128)} %fusion.4), kind=kOutput, calls=%fused_computation.8 | convolution fusion | flops 4835180544 | bytes 20054016 | tf_op jit(solution)/shard_map/dot_general | solution.py:63
  169.9 36.2 %all-reduce.6.cloned.1.call-done = bf16[768,1536]{1,0:T(8,128)(2,1)} async-done(((bf16[768,1536]{1,0:T(8,128)(2,1)}), bf16[768,1536]{1,0:T(8,128)(2,1)}) %all-reduce.6.cloned.1.call-update) | async-done | bytes 2359312 | tf_op jit(solution)/shard_map/psum | solution.py:124
  206.0 2.4 convert_element_type.91
  208.5 2.6 convolution_convert_fusion.3
  211.1 35.2 %reduce-scatter.3.cloned.1.call-done = bf16[384,1024]{1,0:T(8,128)(2,1)} async-done(((bf16[384,4096]{1,0:T(8,128)(2,1)}), bf16[384,1024]{1,0:T(8,128)(2,1)}) %reduce-scatter.3.cloned.1.call-update) | async-done | bytes 786448 | tf_op jit(solution)/shard_map/reduce_scatter | solution.py:67
  246.2 5.5 %all-to-all-start.1 = ((bf16[8,48,1024]{2,1,0:T(8,128)(2,1)}), bf16[8,48,1024]{2,1,0:T(8,128)(2,1)S(1)}, u32[]{:S(2)}, u32[]{:S(2)}) async-start(bf16[8,48,1024]{2,1,0:T(8,128)(2,1)} %bitcast.86), calls=%async_computation.2 | async-start | bytes 1572864 | tf_op jit(solution)/shard_map/all_to_all | solution.py:155
  251.8 0.1 mul.275
  252.1 2.0 copy.50
  254.1 0.9 copy.49
  255.0 2.1 pad_maximum_fusion
  257.1 1.4 fusion.34
  258.5 22.2 %all-to-all-done.1 = bf16[8,48,1024]{2,1,0:T(8,128)(2,1)S(1)} async-done(((bf16[8,48,1024]{2,1,0:T(8,128)(2,1)}), bf16[8,48,1024]{2,1,0:T(8,128)(2,1)S(1)}, u32[]{:S(2)}, u32[]{:S(2)}) %all-to-all-start.1) | async-done | bytes 786464 | tf_op jit(solution)/shard_map/all_to_all | solution.py:155
  280.8 1.0 gather_fusion
  281.8 0.5 reshape.124
  282.3 1.0 multiply_reduce_fusion
  283.3 37.4 %reduce-scatter.5.cloned.1.call-done = bf16[96,1024]{1,0:T(8,128)(2,1)} async-done(((bf16[768,1024]{1,0:T(8,128)(2,1)}), bf16[96,1024]{1,0:T(8,128)(2,1)}) %reduce-scatter.5.cloned.1.call-update) | async-done | bytes 196624 | tf_op jit(solution)/shard_map/reduce_scatter | solution.py:128
  320.7 1.8 add_convert_fusion
  (66 shorter events, 1.2 us)
Async XLA Ops:
  7.2 19.0 %copy-start = (bf16[256,4096]{1,0:T(8,128)(2,1)S(1)}, bf16[256,4096]{1,0:T(8,128)(2,1)}, u32[]{:S(2)}) copy-start(bf16[256,4096]{1,0:T(8,128)(2,1)} %param.36) | copy-start | bytes 6291460
  7.2 6.9 %copy-start.5 = (bf16[96,4096]{1,0:T(8,128)(2,1)S(1)}, bf16[96,4096]{1,0:T(8,128)(2,1)}, u32[]{:S(2)}) copy-start(bf16[96,4096]{1,0:T(8,128)(2,1)} %param.23) | copy-start | bytes 2359300
  7.2 58.3 %all-reduce.4.cloned.1.call-start = ((), (), s32[]{:S(2)}) async-start(), calls=%async_computation.4 | async-start | bytes 1572864 | tf_op jit(solution)/shard_map/psum | solution.py:113
  11.9 7.0 %copy-start.2 = (f32[1,96,1024]{1,2,0:T(8,128)}, f32[1,96,1024]{1,2,0:T(8,128)S(1)}, u32[]{:S(2)}) copy-start(f32[1,96,1024]{1,2,0:T(8,128)S(1)} %copy.42) | copy-start | bytes 1179652
  14.1 4.0 %copy-start.12 = (f32[16,64]{1,0:T(8,128)S(1)}, f32[16,64]{1,0:T(8,128)}, u32[]{:S(2)}) copy-start(f32[16,64]{1,0:T(8,128)} %param.28) | copy-start | bytes 12292
  14.1 4.0 %copy-start.13 = (f32[16,64]{1,0:T(8,128)S(1)}, f32[16,64]{1,0:T(8,128)}, u32[]{:S(2)}) copy-start(f32[16,64]{1,0:T(8,128)} %param.27) | copy-start | bytes 12292
  14.1 4.8 %copy-start.6 = (f32[16,64,16]{1,2,0:T(8,128)S(1)}, f32[16,64,16]{1,2,0:T(8,128)}, u32[]{:S(2)}) copy-start(f32[16,64,16]{1,2,0:T(8,128)} %param.31) | copy-start | bytes 196612
  17.1 3.7 %copy-start.7 = (f32[16,64,16]{1,2,0:T(8,128)S(1)}, f32[16,64,16]{1,2,0:T(8,128)}, u32[]{:S(2)}) copy-start(f32[16,64,16]{1,2,0:T(8,128)} %param.30) | copy-start | bytes 196612
  17.2 5.9 %copy-start.15 = (f32[256]{0:T(256)S(1)}, f32[256]{0:T(256)}, u32[]{:S(2)}) copy-start(f32[256]{0:T(256)} %param.34) | copy-start | bytes 3076
  20.9 6.7 %copy-start.1 = (f32[96,16,64]{0,2,1:T(8,128)}, f32[96,16,64]{0,2,1:T(8,128)S(1)}, u32[]{:S(2)}) copy-start(f32[96,16,64]{0,2,1:T(8,128)S(1)} %fusion.26) | copy-start | bytes 1179652
  26.1 1.5 copy-start.16
  27.5 40.6 %copy-start.8 = (f32[4096]{0:T(1024)S(1)}, f32[4096]{0:T(1024)}, u32[]{:S(2)}) copy-start(f32[4096]{0:T(1024)} %param.25) | copy-start | bytes 49156
  27.6 91.9 %all-gather.5.cloned.1.call-start = ((), (), s32[]{:S(2)}) async-start(), calls=%async_computation.7 | async-start | bytes 1769472 | tf_op jit(solution)/shard_map/all_gather | solution.py:120
  67.2 0.9 copy-start.4
  68.4 5.2 %copy-start.3 = (bf16[96,4096]{1,0:T(8,128)(2,1)}, bf16[96,4096]{1,0:T(8,128)(2,1)S(1)}, u32[]{:S(2)}) copy-start(bf16[96,4096]{1,0:T(8,128)(2,1)S(1)} %fusion.15) | copy-start | bytes 2359300
  69.2 78.9 %all-gather.3.cloned.1.call-start = ((), (), s32[]{:S(2)}) async-start(), calls=%async_computation.5 | async-start | bytes 3932160 | tf_op jit(solution)/shard_map/all_gather | solution.py:148
  70.3 0.6 copy-start.9
  104.6 101.5 %all-reduce.6.cloned.1.call-start = ((), (), s32[]{:S(2)}) async-start(), calls=%async_computation.8 | async-start | bytes 4718592 | tf_op jit(solution)/shard_map/psum | solution.py:124
  125.9 120.4 %reduce-scatter.3.cloned.1.call-start = ((), (), s32[]{:S(2)}) async-start(), calls=%async_computation.6 | async-start | bytes 3932160 | tf_op jit(solution)/shard_map/reduce_scatter | solution.py:67
  169.8 150.9 %reduce-scatter.5.cloned.1.call-start = ((), (), s32[]{:S(2)}) async-start(), calls=%async_computation.9 | async-start | bytes 1769472 | tf_op jit(solution)/shard_map/reduce_scatter | solution.py:128
  206.0 2.4 copy-start.17
  211.0 40.9 %copy-start.11 = (f32[96,2]{0,1:T(2,128)S(1)}, f32[96,2]{0,1:T(2,128)}, u32[]{:S(2)}) copy-start(f32[96,2]{0,1:T(2,128)} %param.38) | copy-start | bytes 2308
  211.0 41.0 %copy-start.14 = (bf16[4096]{0:T(1024)(128)(2,1)S(1)}, bf16[4096]{0:T(1024)(128)(2,1)}, u32[]{:S(2)}) copy-start(bf16[4096]{0:T(1024)(128)(2,1)} %param.45) | copy-start | bytes 24580
  211.1 43.9 %copy-start.10 = (s32[192]{0:T(256)S(1)}, s32[192]{0:T(256)}, u32[]{:S(2)}) copy-start(s32[192]{0:T(256)} %copy-done.9) | copy-start | bytes 2308
  246.2 34.5 %all-to-all-start.1 = ((bf16[8,48,1024]{2,1,0:T(8,128)(2,1)}), bf16[8,48,1024]{2,1,0:T(8,128)(2,1)S(1)}, u32[]{:S(2)}, u32[]{:S(2)}) async-start(bf16[8,48,1024]{2,1,0:T(8,128)(2,1)} %bitcast.86), calls=%async_computation.2 | async-start | bytes 1572864 | tf_op jit(solution)/shard_map/all_to_all | solution.py:155
Sparse Core Ops, SparseCore 0:
  27.7 37.7 all-reduce.3
  69.3 50.0 all-gather.4
  121.0 27.0 all-gather.2
  150.3 55.6 all-reduce.5
  208.4 37.7 reduce-scatter.2
  249.5 71.1 reduce-scatter.4
where the time goes:
time: 330 us; the launch traced here: 329 us
  waiting for transfers between devices  205 us (62%)
  matrix products  44.3 us (13%)
  blocking collectives  30.8 us (9%)
  local copies, waits for them, and re-layouts  16.2 us (5%)
  between operations  14.4 us (4%)
  other arithmetic  12.1 us (4%)
  starting transfers between devices  5.94 us (2%)
    psum x1, waiting for transfers between devices, shards(): mixed = lax.psum(partial_value.astype(jnp.bfloat16), 'tp')  37.6 us
    reduce_scatter x1, waiting for transfers between devices, shards(): lax.psum_scatter(jnp.dot(dense_hidden, dense_down, preferred_element_type...  37.4 us
    psum x1, waiting for transfers between devices, shards(): lax.psum(partial_both.astype(jnp.bfloat16), 'tp').astype(jnp.float32)  36.2 us
    reduce_scatter x1, waiting for transfers between devices, expert_rows(): lax.psum_scatter(partial_value.astype(jnp.bfloat16), 'tp', scatter_dimens...  35.2 us
    all_to_all x1, blocking collectives, shards(): lax.all_to_all(send_part, 'ep', split_axis=0, concat_axis=0, tiled=True)  30.8 us
    all_to_all x1, waiting for transfers between devices, shards(): lax.all_to_all(answered, 'ep', split_axis=0, concat_axis=0, tiled=True)  22.2 us
    all_gather x1, waiting for transfers between devices, shards(): lax.all_gather(lax.all_to_all(send_part, 'ep', split_axis=0, concat_axis=...  22 us
    all_gather x1, waiting for transfers between devices, shards(): lax.all_gather(own_cols, 'ep', axis=0, tiled=True)  14.9 us
  transfers between devices with their start and end apart: 7, of which 7 were waited for; matrix products, arithmetic and copies ran while one was open for 14% of the time, Pallas kernels for 0%

commit v1 on v0

--- a/solution.py
+++ b/solution.py
@@ -152,7 +152,15 @@
         tiled=True,
     )
     answered = expert_rows(full_rows, expert_gate[0], expert_up[0], expert_down[0], part_width)
-    returned = lax.all_to_all(answered, "ep", split_axis=0, concat_axis=0, tiled=True)
+    ways, here = (lax.axis_size("ep"), lax.axis_index("ep"))
+    width_2 = answered.shape[0] // ways
+    turned = jnp.roll(answered, -here * width_2, axis=0)
+    got = [lax.slice_in_dim(turned, 0, width_2, axis=0)]
+    for far in range(1, ways):
+        sent = lax.slice_in_dim(turned, far * width_2, (far + 1) * width_2, axis=0)
+        got.append(lax.ppermute(sent, "ep", [(d, (d + far) % ways) for d in range(ways)]))
+    line = jnp.concatenate(got[::-1], axis=0)
+    returned = jnp.roll(line, (here + 1) * got[0].shape[0], axis=0)
     picked_rows = returned.reshape(ep_count * capacity, part_width)[target]
     picked_rows = picked_rows.reshape(seq_count, top_count, part_width).astype(jnp.float32)
     route_weights = jax.nn.softmax(route_logits, axis=-1)

time: 330 us -> 324 us (0.982)
  local copies, waits for them, and re-layouts: 16.2 us -> 7.75 us
  starting transfers between devices: 5.94 us -> 11 us
    all_to_all x1 -> x0, waiting for transfers between devices: 22.2 us -> none  [shards(): lax.all_to_all(answered, 'ep', split_axis=0, concat_axis=0, tiled=True)]
    ppermute x0 -> x7, waiting for transfers between devices: none -> 19.9 us  [shards(): lax.ppermute(sent, 'ep', [(d, (d + far) % ways) for d in range(ways)])]
    ppermute x0 -> x7, starting transfers between devices: none -> 10.6 us  [shards(): lax.ppermute(sent, 'ep', [(d, (d + far) % ways) for d in range(ways)])]
    all_to_all x1 -> x0, starting transfers between devices: 5.51 us -> none  [shards(): lax.all_to_all(answered, 'ep', split_axis=0, concat_axis=0, tiled=True)]
    reduce_scatter x1, waiting for transfers between devices: 35.2 us -> 31.5 us  [expert_rows(): lax.psum_scatter(partial_value.astype(jnp.bfloat16), 'tp', scatter_dimens...]
  transfers between devices with their start and end apart: 7 -> 13, of which waited for: 7 -> 10; matrix products, arithmetic and copies ran while one was open for 14% -> 14% of each run, Pallas kernels for 0% -> 0%
where the time goes in v1:
time: 324 us
  waiting for transfers between devices  203 us (63%)
  matrix products  43.9 us (14%)
  blocking collectives  30.8 us (10%)
  between operations  14.6 us (5%)
  other arithmetic  12.4 us (4%)
  starting transfers between devices  11 us (3%)
  local copies, waits for them, and re-layouts  7.75 us (2%)
    reduce_scatter x1, waiting for transfers between devices, shards(): lax.psum_scatter(jnp.dot(dense_hidden, dense_down, preferred_element_type...  39.4 us
    psum x1, waiting for transfers between devices, shards(): mixed = lax.psum(partial_value.astype(jnp.bfloat16), 'tp')  37.6 us
    psum x1, waiting for transfers between devices, shards(): lax.psum(partial_both.astype(jnp.bfloat16), 'tp').astype(jnp.float32)  36.2 us
    reduce_scatter x1, waiting for transfers between devices, expert_rows(): lax.psum_scatter(partial_value.astype(jnp.bfloat16), 'tp', scatter_dimens...  31.5 us
    all_to_all x1, blocking collectives, shards(): lax.all_to_all(send_part, 'ep', split_axis=0, concat_axis=0, tiled=True)  30.8 us
    all_gather x1, waiting for transfers between devices, shards(): lax.all_gather(lax.all_to_all(send_part, 'ep', split_axis=0, concat_axis=...  21.8 us
    ppermute x7, waiting for transfers between devices, shards(): lax.ppermute(sent, 'ep', [(d, (d + far) % ways) for d in range(ways)])  19.9 us
    all_gather x1, waiting for transfers between devices, shards(): lax.all_gather(own_cols, 'ep', axis=0, tiled=True)  17.1 us
  transfers between devices with their start and end apart: 13, of which 10 were waited for; matrix products, arithmetic and copies ran while one was open for 14% of the time, Pallas kernels for 0%

profile of v1, /device:TPU:0, one launch (start us, length us, event | category | flops | bytes accessed | tf_op | source)
XLA Modules:
  0.0 323.9 jit_solution(3993747818430432152)
XLA Ops:
  7.2 0.8 exp.20
  8.0 1.2 fusion.72
  9.2 0.2 copy.42
  9.4 1.0 copy.43
  10.4 1.4 fusion.16
  11.9 2.4 convolution_convert_fusion.4
  14.6 1.8 fusion.26
  16.4 2.0 fusion.27
  18.5 1.5 fusion.73
  20.0 1.5 fusion.30
  21.5 1.4 convolution_convert_fusion.1
  23.2 37.6 %all-reduce.4.cloned.1.call-done = bf16[96,4096]{1,0:T(8,128)(2,1)} async-done(((bf16[96,4096]{1,0:T(8,128)(2,1)}), bf16[96,4096]{1,0:T(8,128)(2,1)}) %all-reduce.4.cloned.1.call-update) | async-done | bytes 786448 | tf_op jit(solution)/shard_map/psum | solution.py:113
  60.8 1.7 fusion.13
  62.6 0.3 fusion.15
  62.9 0.7 constant_dynamic-slice_fusion
  63.7 0.6 reduce-window.6
  64.2 0.2 slice_reduce_fusion
  65.0 1.0 convolution_convert_fusion
  66.1 30.8 %all_to_all.5 = bf16[8,48,1024]{2,1,0:T(8,128)(2,1)} all-to-all(bf16[8,48,1024]{2,1,0:T(8,128)(2,1)S(1)} %constant_dynamic-slice_fusion.1), channel_id=1, replica_groups=mesh['ep'=8,'tp'=4] {'ep'}, dimensions={0} | all-to-all | bytes 1572864 | tf_op jit(solution)/shard_map/all_to_all | solution.py:149
  96.9 17.1 %all-gather.5.cloned.1.call-done = bf16[768,1024]{1,0:T(8,128)(2,1)} async-done(((bf16[96,1024]{1,0:T(8,128)(2,1)}), bf16[768,1024]{1,0:T(8,128)(2,1)}) %all-gather.5.cloned.1.call-update) | async-done | bytes 1572880 | tf_op jit(solution)/shard_map/all_gather | solution.py:120
  114.0 6.4 %convolution_convert_fusion.2 = bf16[768,1536]{1,0:T(8,128)(2,1)} fusion(bf16[768,1024]{1,0:T(8,128)(2,1)} %all-gather.5.cloned.1.call-done, bf16[1024,768]{1,0:T(8,128)(2,1)} %param.45, bf16[1024,768]{1,0:T(8,128)(2,1)} %param.44), kind=kOutput, calls=%fused_computation.10 | convolution fusion | flops 2423390208 | bytes 7077888 | tf_op jit(solution)/shard_map/dot_general | solution.py:119
  120.4 0.2 reduce-scatter.3.cloned.1.call-start
  120.6 21.8 %all-gather.3.cloned.1.call-done = bf16[8,48,4096]{2,1,0:T(8,128)(2,1)} async-done(((bf16[8,48,1024]{2,1,0:T(8,128)(2,1)}), bf16[8,48,4096]{2,1,0:T(8,128)(2,1)}) %all-gather.3.cloned.1.call-update) | async-done | bytes 3145744 | tf_op jit(solution)/shard_map/all_gather | solution.py:148
  142.5 7.4 %fusion.4 = f32[384,768]{1,0:T(8,128)} fusion(bf16[384,4096]{1,0:T(8,128)(2,1)} %bitcast.89, bf16[1,4096,768]{2,1,0:T(8,128)(2,1)} %param.41), kind=kOutput, calls=%fused_computation.5 | convolution fusion | flops 2415919104 | bytes 10616832 | tf_op jit(solution)/shard_map/dot_general | solution.py:59
  149.8 14.3 %fusion.6 = bf16[384,4096]{1,0:T(8,128)(2,1)} fusion(bf16[1,768,4096]{2,1,0:T(8,128)(2,1)} %param.43, bf16[384,4096]{1,0:T(8,128)(2,1)} %bitcast.90, bf16[1,4096,768]{2,1,0:T(8,128)(2,1)} %param.42, f32[384,768]{1,0:T(8,128)} %fusion.4), kind=kOutput, calls=%fused_computation.8 | convolution fusion | flops 4835180544 | bytes 20054016 | tf_op jit(solution)/shard_map/dot_general | solution.py:63
  164.2 36.2 %all-reduce.6.cloned.1.call-done = bf16[768,1536]{1,0:T(8,128)(2,1)} async-done(((bf16[768,1536]{1,0:T(8,128)(2,1)}), bf16[768,1536]{1,0:T(8,128)(2,1)}) %all-reduce.6.cloned.1.call-update) | async-done | bytes 2359312 | tf_op jit(solution)/shard_map/psum | solution.py:124
  200.4 2.3 convert_element_type.91
  202.7 4.0 %convolution_convert_fusion.3 = bf16[768,1024]{1,0:T(8,128)(2,1)} fusion(bf16[768,1024]{1,0:T(8,128)(2,1)} %param.46, f32[768,1536]{1,0:T(8,128)S(1)} %convert_element_type.91), kind=kOutput, calls=%fused_computation.21 | convolution fusion | flops 1212284928 | bytes 7864320 | tf_op jit(solution)/shard_map/dot_general | solution.py:129
  207.0 0.7 copy.45
  208.2 1.0 pad_maximum_fusion
  209.2 31.5 %reduce-scatter.3.cloned.1.call-done = bf16[384,1024]{1,0:T(8,128)(2,1)} async-done(((bf16[384,4096]{1,0:T(8,128)(2,1)}), bf16[384,1024]{1,0:T(8,128)(2,1)}) %reduce-scatter.3.cloned.1.call-update) | async-done | bytes 786448 | tf_op jit(solution)/shard_map/reduce_scatter | solution.py:67
  240.6 1.4 fusion.36
  242.1 4.3 %collective-permute-start = (bf16[1,48,1024]{2,1,0:T(8,128)(2,1)S(1)}, bf16[1,48,1024]{2,1,0:T(8,128)(2,1)S(1)}, u32[]{:S(2)}, u32[]{:S(2)}) collective-permute-start(bf16[1,48,1024]{2,1,0:T(8,128)(2,1)S(1)} %get-tuple-element.11), channel_id=1, source_target_pairs={{0,28},{4,0},{8,4},{12,8},{16,12},{20,16},{24,20},{28,24},{1,29},{... | collective-permute-start | bytes 294920 | tf_op jit(solution)/shard_map/ppermute | solution.py:161
  246.4 0.3 fusion.34
  246.7 0.5 collective-permute-start.1
  247.2 3.0 collective-permute-start.3
  250.2 1.9 collective-permute-start.5
  252.1 0.4 collective-permute-done.1
  252.6 0.8 collective-permute-start.6
  253.4 2.5 collective-permute-done.2
  256.0 12.9 %collective-permute-done.3 = bf16[1,48,1024]{2,1,0:T(8,128)(2,1)S(1)} collective-permute-done((bf16[1,48,1024]{2,1,0:T(8,128)(2,1)S(1)}, bf16[1,48,1024]{2,1,0:T(8,128)(2,1)S(1)}, u32[]{:S(2)}, u32[]{:S(2)}) %collective-permute-start.3) | collective-permute-done | bytes 98336 | tf_op jit(solution)/shard_map/ppermute | solution.py:161
  268.9 4.0 %collective-permute-done.4 = bf16[1,48,1024]{2,1,0:T(8,128)(2,1)S(1)} collective-permute-done((bf16[1,48,1024]{2,1,0:T(8,128)(2,1)S(1)}, bf16[1,48,1024]{2,1,0:T(8,128)(2,1)S(1)}, u32[]{:S(2)}, u32[]{:S(2)}) %collective-permute-start.4) | collective-permute-done | bytes 98336 | tf_op jit(solution)/shard_map/ppermute | solution.py:161
  273.0 0.3 fusion.35
  273.3 1.0 gather_fusion
  274.3 0.5 reshape.124
  274.8 1.0 multiply_reduce_fusion
  275.9 39.4 %reduce-scatter.5.cloned.1.call-done = bf16[96,1024]{1,0:T(8,128)(2,1)} async-done(((bf16[768,1024]{1,0:T(8,128)(2,1)}), bf16[96,1024]{1,0:T(8,128)(2,1)}) %reduce-scatter.5.cloned.1.call-update) | async-done | bytes 196624 | tf_op jit(solution)/shard_map/reduce_scatter | solution.py:128
  315.2 1.8 add_convert_fusion
  (83 shorter events, 2.3 us)
Async XLA Ops:
  7.2 14.4 %copy-start = (bf16[256,4096]{1,0:T(8,128)(2,1)S(1)}, bf16[256,4096]{1,0:T(8,128)(2,1)}, u32[]{:S(2)}) copy-start(bf16[256,4096]{1,0:T(8,128)(2,1)} %param.38) | copy-start | bytes 6291460
  7.2 53.6 %all-reduce.4.cloned.1.call-start = ((), (), s32[]{:S(2)}) async-start(), calls=%async_computation.3 | async-start | bytes 1572864 | tf_op jit(solution)/shard_map/psum | solution.py:113
  8.0 3.9 %copy-start.14 = (f32[4096]{0:T(1024)S(1)}, f32[4096]{0:T(1024)}, u32[]{:S(2)}) copy-start(f32[4096]{0:T(1024)} %param.26) | copy-start | bytes 49156
  9.4 5.1 %copy-start.2 = (f32[1,96,1024]{1,2,0:T(8,128)}, f32[1,96,1024]{1,2,0:T(8,128)S(1)}, u32[]{:S(2)}) copy-start(f32[1,96,1024]{1,2,0:T(8,128)S(1)} %copy.42) | copy-start | bytes 1179652
  10.4 4.0 %copy-start.9 = (f32[16,64]{1,0:T(8,128)S(1)}, f32[16,64]{1,0:T(8,128)}, u32[]{:S(2)}) copy-start(f32[16,64]{1,0:T(8,128)} %param.30) | copy-start | bytes 12292
  10.4 4.0 %copy-start.10 = (f32[16,64]{1,0:T(8,128)S(1)}, f32[16,64]{1,0:T(8,128)}, u32[]{:S(2)}) copy-start(f32[16,64]{1,0:T(8,128)} %param.29) | copy-start | bytes 12292
  10.4 4.1 %copy-start.4 = (f32[16,64,16]{1,2,0:T(8,128)S(1)}, f32[16,64,16]{1,2,0:T(8,128)}, u32[]{:S(2)}) copy-start(f32[16,64,16]{1,2,0:T(8,128)} %param.33) | copy-start | bytes 196612
  10.4 4.1 %copy-start.5 = (f32[16,64,16]{1,2,0:T(8,128)S(1)}, f32[16,64,16]{1,2,0:T(8,128)}, u32[]{:S(2)}) copy-start(f32[16,64,16]{1,2,0:T(8,128)} %param.32) | copy-start | bytes 196612
  14.3 4.1 %copy-start.12 = (f32[256]{0:T(256)S(1)}, f32[256]{0:T(256)}, u32[]{:S(2)}) copy-start(f32[256]{0:T(256)} %param.36) | copy-start | bytes 3076
  21.4 1.5 copy-start.13
  22.9 39.7 %copy-start.7 = (f32[4096]{0:T(1024)S(1)}, f32[4096]{0:T(1024)}, u32[]{:S(2)}) copy-start(f32[4096]{0:T(1024)} %param.27) | copy-start | bytes 49156
  22.9 91.1 %all-gather.5.cloned.1.call-start = ((), (), s32[]{:S(2)}) async-start(), calls=%async_computation.6 | async-start | bytes 1769472 | tf_op jit(solution)/shard_map/all_gather | solution.py:120
  62.6 3.4 %copy-start.3 = (bf16[96,4096]{1,0:T(8,128)(2,1)}, bf16[96,4096]{1,0:T(8,128)(2,1)S(1)}, u32[]{:S(2)}) copy-start(bf16[96,4096]{1,0:T(8,128)(2,1)S(1)} %get-tuple-element.4) | copy-start | bytes 2359300
  63.6 78.9 %all-gather.3.cloned.1.call-start = ((), (), s32[]{:S(2)}) async-start(), calls=%async_computation.4 | async-start | bytes 3932160 | tf_op jit(solution)/shard_map/all_gather | solution.py:148
  96.9 103.5 %all-reduce.6.cloned.1.call-start = ((), (), s32[]{:S(2)}) async-start(), calls=%async_computation.7 | async-start | bytes 4718592 | tf_op jit(solution)/shard_map/psum | solution.py:124
  120.4 120.2 %reduce-scatter.3.cloned.1.call-start = ((), (), s32[]{:S(2)}) async-start(), calls=%async_computation.5 | async-start | bytes 3932160 | tf_op jit(solution)/shard_map/reduce_scatter | solution.py:67
  164.2 151.1 %reduce-scatter.5.cloned.1.call-start = ((), (), s32[]{:S(2)}) async-start(), calls=%async_computation.8 | async-start | bytes 1769472 | tf_op jit(solution)/shard_map/reduce_scatter | solution.py:128
  202.7 4.3 %copy-start.8 = (f32[96,2]{0,1:T(2,128)S(1)}, f32[96,2]{0,1:T(2,128)}, u32[]{:S(2)}) copy-start(f32[96,2]{0,1:T(2,128)} %param.40) | copy-start | bytes 2308
  202.7 5.0 %copy-start.11 = (bf16[4096]{0:T(1024)(128)(2,1)S(1)}, bf16[4096]{0:T(1024)(128)(2,1)}, u32[]{:S(2)}) copy-start(bf16[4096]{0:T(1024)(128)(2,1)} %param.47) | copy-start | bytes 24580
  242.1 8.1 %collective-permute-start = (bf16[1,48,1024]{2,1,0:T(8,128)(2,1)S(1)}, bf16[1,48,1024]{2,1,0:T(8,128)(2,1)S(1)}, u32[]{:S(2)}, u32[]{:S(2)}) collective-permute-start(bf16[1,48,1024]{2,1,0:T(8,128)(2,1)S(1)} %get-tuple-element.11), channel_id=1, source_target_pairs={{0,28},{4,0},{8,4},{12,8},{16,12},{20,16},{24,20},{28,24},{1,29},{... | collective-permute-start | bytes 294920 | tf_op jit(solution)/shard_map/ppermute | solution.py:161
  246.7 5.9 %collective-permute-start.1 = (bf16[1,48,1024]{2,1,0:T(8,128)(2,1)S(1)}, bf16[1,48,1024]{2,1,0:T(8,128)(2,1)S(1)}, u32[]{:S(2)}, u32[]{:S(2)}) collective-permute-start(bf16[1,48,1024]{2,1,0:T(8,128)(2,1)S(1)} %get-tuple-element.10), channel_id=1, source_target_pairs={{0,24},{4,28},{8,0},{12,4},{16,8},{20,12},{24,16},{28,20},{1,25},{... | collective-permute-start | bytes 294920 | tf_op jit(solution)/shard_map/ppermute | solution.py:161
  247.2 8.7 %collective-permute-start.2 = (bf16[1,48,1024]{2,1,0:T(8,128)(2,1)S(1)}, bf16[1,48,1024]{2,1,0:T(8,128)(2,1)S(1)}, u32[]{:S(2)}, u32[]{:S(2)}) collective-permute-start(bf16[1,48,1024]{2,1,0:T(8,128)(2,1)S(1)} %get-tuple-element.9), channel_id=1, source_target_pairs={{0,20},{4,24},{8,28},{12,0},{16,4},{20,8},{24,12},{28,16},{1,21},{... | collective-permute-start | bytes 294920 | tf_op jit(solution)/shard_map/ppermute | solution.py:161
  247.2 21.6 %collective-permute-start.3 = (bf16[1,48,1024]{2,1,0:T(8,128)(2,1)S(1)}, bf16[1,48,1024]{2,1,0:T(8,128)(2,1)S(1)}, u32[]{:S(2)}, u32[]{:S(2)}) collective-permute-start(bf16[1,48,1024]{2,1,0:T(8,128)(2,1)S(1)} %get-tuple-element.8), channel_id=1, source_target_pairs={{0,16},{4,20},{8,24},{12,28},{16,0},{20,4},{24,8},{28,12},{1,17},{... | collective-permute-start | bytes 294920 | tf_op jit(solution)/shard_map/ppermute | solution.py:161
  250.2 22.7 %collective-permute-start.4 = (bf16[1,48,1024]{2,1,0:T(8,128)(2,1)S(1)}, bf16[1,48,1024]{2,1,0:T(8,128)(2,1)S(1)}, u32[]{:S(2)}, u32[]{:S(2)}) collective-permute-start(bf16[1,48,1024]{2,1,0:T(8,128)(2,1)S(1)} %get-tuple-element.7), channel_id=1, source_target_pairs={{0,12},{4,16},{8,20},{12,24},{16,28},{20,0},{24,4},{28,8},{1,13},{... | collective-permute-start | bytes 294920 | tf_op jit(solution)/shard_map/ppermute | solution.py:161
  250.2 22.7 %collective-permute-start.5 = (bf16[1,48,1024]{2,1,0:T(8,128)(2,1)S(1)}, bf16[1,48,1024]{2,1,0:T(8,128)(2,1)S(1)}, u32[]{:S(2)}, u32[]{:S(2)}) collective-permute-start(bf16[1,48,1024]{2,1,0:T(8,128)(2,1)S(1)} %get-tuple-element.6), channel_id=1, source_target_pairs={{0,8},{4,12},{8,16},{12,20},{16,24},{20,28},{24,0},{28,4},{1,9},{5... | collective-permute-start | bytes 294920 | tf_op jit(solution)/shard_map/ppermute | solution.py:161
  252.6 20.4 %collective-permute-start.6 = (bf16[1,48,1024]{2,1,0:T(8,128)(2,1)S(1)}, bf16[1,48,1024]{2,1,0:T(8,128)(2,1)S(1)}, u32[]{:S(2)}, u32[]{:S(2)}) collective-permute-start(bf16[1,48,1024]{2,1,0:T(8,128)(2,1)S(1)} %get-tuple-element.5), channel_id=1, source_target_pairs={{0,4},{4,8},{8,12},{12,16},{16,20},{20,24},{24,28},{28,0},{1,5},{5... | collective-permute-start | bytes 294920 | tf_op jit(solution)/shard_map/ppermute | solution.py:161
  273.3 1.5 copy-start.6
  273.3 43.8 %copy-start.1 = (bf16[256,4096]{1,0:T(8,128)(2,1)S(1)}, bf16[256,4096]{1,0:T(8,128)(2,1)}, u32[]{:S(2)}) copy-start(bf16[256,4096]{1,0:T(8,128)(2,1)} %param.38) | copy-start | bytes 6291460
Sparse Core Ops, SparseCore 0:
  23.1 37.7 all-reduce.3
  63.7 50.2 all-gather.4
  115.6 26.8 all-gather.2
  144.7 55.6 all-reduce.5
  202.8 37.7 reduce-scatter.2
  243.9 71.3 reduce-scatter.4
